TPU v7x, 32 devices: a whole 2x2x4 slice. The times are simulated.
32 devices in a mesh: grp: 2 (over y), ep: 4 (over z), tp: 4 (over x, core).
Axes of the slice: x: 2, y: 2, z: 4, core: 2. Of those that a mesh axis runs over, the one named last changes fastest.
Arguments:
- mix_input: bfloat16 [2048, 2048], P(('grp', 'ep'), 'tp'), parts along dimension 0, may hold values from -6 to 6
- group_weight: bfloat16 [16, 128, 128], replicated, may hold values from -0.5 to 0.5
- pool_gain: float32 [2048], replicated, may hold values from 0.1 to 1.9
- branch_weight: bfloat16 [2048, 2048], P('tp'), may hold values from -0.125 to 0.125
- exp_input: bfloat16 [1024, 2048], P(('grp', 'ep')), parts along dimension 0, may hold values from -6 to 6
- norm_gain: float32 [2048], replicated, may hold values from 0.1 to 1.9
- routes: int32 [1024, 2], P(('grp', 'ep')), parts along dimension 0, may hold values from 0 to 3, all different within a row; in each aligned block of 128 rows (0 to 127, 128 to 255, ...) at most 96 rows name the same one
- route_weights: float32 [1024, 2], P(('grp', 'ep')), parts along dimension 0, may hold values from 0.25 to 1
- gate_weight: bfloat16 [4, 2048, 3584], P('ep', None, 'tp'), may hold values from -0.125 to 0.125
- up_weight: bfloat16 [4, 2048, 3584], P('ep', None, 'tp'), may hold values from -0.125 to 0.125
- down_weight: bfloat16 [4, 3584, 2048], P('ep', 'tp'), may hold values from -0.09375 to 0.09375
Outputs:
- mix_out: bfloat16 [2048, 2048], P(('grp', 'ep'), 'tp'), parts along dimension 0
- exp_out: bfloat16 [1024, 2048], P(('grp', 'ep'), 'tp'), parts along dimension 0
There are 2 independent parts, one for each index of `grp`. A program takes and returns all parts, laid end to end along the dimension named above; an argument that names none is the same for every part. Nothing has to cross between parts.
Inputs may be any that keep to these rules, and one draw needn't show every extreme that they name: `routes`: the 2 experts of a token differ. Among the 128 tokens of one index of ep no expert is named by more than 96 of them, a bound that some block reaches.
All inputs are finite; a program needn't handle non-finite values.
Results may differ from a plain program's by a relative error of at most 0.018.
Values may be sent and summed in bfloat16 or wider, within the bound.
No kernel may reach another device: no remote copies, remote signals or barrier semaphores. Data moves between devices by JAX's collectives and lax.ppermute only.
A program may use at most 64 MiB of HBM per device.

v0:
```python
import jax
import jax.numpy as jnp
from jax import lax
from jax.sharding import PartitionSpec as P

windows = (2, 4, 8, 16)
epsilon = 1e-06


def shifted(block, axis, distance):
    devices = range(lax.axis_size(axis))
    route = [(i - distance, i) for i in devices if i - distance in devices]
    return lax.ppermute(block, axis, route)


def trailing_sums(extended, rows):
    span_two = extended[1:] + extended[:-1]
    span_four = span_two[2:] + span_two[:-2]
    span_eight = span_four[4:] + span_four[:-4]
    span_sixteen = span_eight[8:] + span_eight[:-8]
    return [span_two[-rows:], span_four[-rows:], span_eight[-rows:], span_sixteen]


def pooled_deviation(extended, positions, group_ids, group_width, rows):
    sums = trailing_sums(extended, rows)
    current = extended[-rows:]
    window_id = jnp.repeat(group_ids % 4, group_width)
    result = jnp.zeros_like(current)
    for window_level, window_len in enumerate(windows):
        counted = jnp.minimum(positions + 1, window_len).astype(jnp.float32)[:, None]
        result = jnp.where(
            window_id[None, :] == window_level, sums[window_level] / counted - current, result
        )
    return result


def on_device(
    mix_input,
    group_weight,
    pool_gain,
    branch_weight,
    exp_input,
    norm_gain,
    routes,
    route_weights,
    gate_weight,
    up_weight,
    down_weight,
):
    tp_rank = lax.axis_index("tp")
    ep_rank = lax.axis_index("ep")
    rows_mix, channels = mix_input.shape
    group_width = group_weight.shape[1]
    group_count = channels // group_width
    first_group = tp_rank * group_count
    last_rows = mix_input[rows_mix - 15 :]
    before = shifted(last_rows, "ep", 1)
    extended = jnp.concatenate([before, mix_input], axis=0).astype(jnp.float32)
    positions = ep_rank * rows_mix + jnp.arange(rows_mix, dtype=jnp.int32)
    group_ids = first_group + jnp.arange(group_count, dtype=jnp.int32)
    deviation = pooled_deviation(extended, positions, group_ids, group_width, rows_mix).astype(
        jnp.bfloat16
    )
    own_groups = lax.dynamic_slice_in_dim(group_weight, first_group, group_count, 0)
    grouped = jnp.einsum(
        "rgc,gcd->rgd",
        deviation.reshape(rows_mix, group_count, group_width),
        own_groups,
        preferred_element_type=jnp.float32,
    ).reshape(rows_mix, channels)
    own_gain = lax.dynamic_slice_in_dim(pool_gain, first_group * group_width, channels, 0)
    pooled = (grouped * own_gain).astype(jnp.bfloat16)
    tok_rows, width = exp_input.shape
    columns = width // lax.axis_size("tp")
    experts_all = lax.axis_size("ep")
    capacity = 3 * tok_rows // experts_all
    floated = exp_input.astype(jnp.float32)
    normed = (
        floated
        * lax.rsqrt(jnp.mean(floated * floated, axis=1, keepdims=True) + epsilon)
        * norm_gain
    ).astype(jnp.bfloat16)
    flat_expert = routes.reshape(-1)
    assignments = flat_expert.shape[0]
    onehot = (flat_expert[:, None] == jnp.arange(experts_all, dtype=jnp.int32)[None, :]).astype(
        jnp.int32
    )
    slot_rank = jnp.sum((jnp.cumsum(onehot, axis=0) - onehot) * onehot, axis=1)
    slot_index = flat_expert * capacity + slot_rank
    token_of = jnp.arange(assignments, dtype=jnp.int32) // routes.shape[1]
    slot_token = (
        jnp.full((experts_all * capacity,), tok_rows, jnp.int32).at[slot_index].set(token_of)
    )
    padded = jnp.concatenate([normed, jnp.zeros((1, width), jnp.bfloat16)], axis=0)
    w_gate = gate_weight[0]
    w_up = up_weight[0]
    w_down = down_weight[0]
    arrived_rows = experts_all * capacity
    own_columns = lax.dynamic_slice_in_dim(padded, tp_rank * columns, columns, 1)
    outgoing = own_columns[slot_token].reshape(experts_all, capacity, columns)
    arrived = lax.all_to_all(outgoing, "ep", split_axis=0, concat_axis=0, tiled=True).reshape(
        arrived_rows, columns
    )
    section = lax.all_gather(arrived, "tp", axis=1, tiled=True)
    gate_pre = jnp.dot(section, w_gate, preferred_element_type=jnp.float32)
    up_pre = jnp.dot(section, w_up, preferred_element_type=jnp.float32)
    hidden = (jax.nn.silu(gate_pre) * up_pre).astype(jnp.bfloat16)
    weight_cols = branch_weight
    mix_sum = lax.psum_scatter(
        lax.dot_general(
            weight_cols, pooled, (((0,), (1,)), ((), ())), preferred_element_type=jnp.float32
        ).astype(jnp.bfloat16),
        "tp",
        scatter_dimension=0,
        tiled=True,
    )
    weight_cols = w_down
    exp_sum = lax.psum_scatter(
        lax.dot_general(
            weight_cols, hidden, (((0,), (1,)), ((), ())), preferred_element_type=jnp.float32
        ).astype(jnp.bfloat16),
        "tp",
        scatter_dimension=0,
        tiled=True,
    )
    mix_out = mix_sum.T
    results = exp_sum.reshape(columns, experts_all, capacity)
    returned = lax.all_to_all(results, "ep", split_axis=1, concat_axis=1, tiled=True).reshape(
        columns, experts_all * capacity
    )
    picked = returned[:, slot_index].astype(jnp.float32)
    weighted = picked * route_weights.reshape(-1)[None, :]
    combined = jnp.sum(weighted.reshape(columns, tok_rows, routes.shape[1]), axis=2)
    exp_out = combined.T.astype(jnp.bfloat16)
    return (mix_out, exp_out)


def solution(mesh):
    return jax.shard_map(
        on_device,
        mesh=mesh,
        in_specs=(
            P(("grp", "ep"), "tp"),
            P(),
            P(),
            P("tp", None),
            P(("grp", "ep"), None),
            P(),
            P(("grp", "ep"), None),
            P(("grp", "ep"), None),
            P("ep", None, "tp"),
            P("ep", None, "tp"),
            P("ep", "tp", None),
        ),
        out_specs=(P(("grp", "ep"), "tp"), P(("grp", "ep"), "tp")),
        check_vma=False,
    )
```

profile of v0, /device:TPU:0, one launch (start us, length us, event | category | flops | bytes accessed | tf_op | source)
XLA Modules:
  0.0 130.7 jit_solution(4550041975561271826)
XLA Ops:
  7.2 0.9 copy.21
  8.2 0.1 eq.97
  8.3 0.1 eq.93
  8.4 0.7 broadcast_multiply_fusion
  9.1 1.2 fusion.19
  10.4 1.2 reduce-window.6
  11.6 0.1 slice.72
  11.7 0.1 copy.23
  11.8 0.1 copy.24
  11.9 0.1 add_bitcast_fusion
  12.0 0.1 copy.20
  12.1 0.1 mul.84
  12.3 1.4 %scatter_custom_fusion = s32[384]{0:T(512)S(1)} fusion(s32[256]{0:T(256)S(1)} %bitcast.86, s32[256]{0:T(256)S(1)} %and_select_fusion, s32[]{:T(128)} %constant.80.clone.1), kind=kCustom, calls=%fused_computation.66 | custom fusion | bytes 1540 | tf_op jit(solution)/shard_map/scatter | solution.py:92
  13.7 1.2 fusion.21
  15.0 2.1 %gather_fusion = bf16[384,512]{1,0:T(8,128)(2,1)S(1)} fusion(bf16[129,512]{1,0:T(8,128)(2,1)S(1)} %pad_dynamic-slice_fusion, s32[1024]{0:T(1024)S(1)} %pad_clamp_fusion.1), kind=kCustom, calls=%fused_computation | custom fusion | bytes 787968 | tf_op jit(solution)/shard_map/gather | solution.py:100
  17.1 17.9 %all_to_all.10 = bf16[4,96,512]{2,1,0:T(8,128)(2,1)} all-to-all(bf16[4,96,512]{2,1,0:T(8,128)(2,1)S(1)} %bitcast.83), channel_id=1, replica_groups=mesh['grp'=2,'ep'=4,'tp'=4] {'ep'}, dimensions={0} | all-to-all | bytes 786432 | tf_op jit(solution)/shard_map/all_to_all | solution.py:101
  35.1 2.1 %collective-permute-start = (bf16[15,512]{1,0:T(8,128)(2,1)S(1)}, bf16[15,512]{1,0:T(8,128)(2,1)S(1)}, u32[]{:S(2)}, u32[]{:S(2)}) collective-permute-start(bf16[15,512]{1,0:T(8,128)(2,1)S(1)} %slice.43), channel_id=1, source_target_pairs={{0,4},{4,8},{8,12},{1,5},{5,9},{9,13},{2,6},{6,10},{10,14},{3,7},{... | collective-permute-start | bytes 46088 | tf_op jit(solution)/shard_map/ppermute | solution.py:13
  37.2 16.7 %all-gather.2.cloned.1.call-done = bf16[384,2048]{1,0:T(8,128)(2,1)} async-done(((bf16[384,512]{1,0:T(8,128)(2,1)}), bf16[384,2048]{1,0:T(8,128)(2,1)}) %all-gather.2.cloned.1.call-update) | async-done | bytes 1572880 | tf_op jit(solution)/shard_map/all_gather | solution.py:104
  53.9 5.4 %fusion.4 = f32[384,896]{1,0:T(8,128)} fusion(bf16[384,2048]{1,0:T(8,128)(2,1)} %all-gather.2.cloned.1.call-done, bf16[1,2048,896]{2,1,0:T(8,128)(2,1)} %param.19), kind=kOutput, calls=%fused_computation.7 | convolution fusion | flops 1409286144 | bytes 6619136 | tf_op jit(solution)/shard_map/dot_general | solution.py:105
  59.3 8.6 %fusion.9 = bf16[2048,384]{0,1:T(8,128)(2,1)} fusion(bf16[1,896,2048]{2,1,0:T(8,128)(2,1)} %param.21, bf16[384,2048]{1,0:T(8,128)(2,1)} %all-gather.2.cloned.1.call-done, bf16[1,2048,896]{2,1,0:T(8,128)(2,1)} %param.20, f32[384,896]{1,0:T(8,128)} %fusion.4), kind=kOutput, calls=%fused_computation.10 | convolution fusion | flops 2821423104 | bytes 11862016 | tf_op jit(solution)/shard_map/dot_general | solution.py:119
  68.4 0.8 dynamic_slice.10
  69.4 1.5 %fusion.35 = f32[4,128,256]{2,1,0:T(8,128)S(1)} fusion(bf16[16,128,128]{2,1,0:T(8,128)(2,1)} %param.12, s32[]{:T(128)S(6)} %select_n.46, f32[256]{0:T(256)S(1)} %get-tuple-element.2, f32[270,512]{1,0:T(8,128)S(1)} %slice_add_fusion.1, pred[512]{0:T(512)(128)(4,1)S(1)} %broadcast_bitcast_fusion, f32[256]{0:T(256)S(1)} %get-tuple-element.3, ...), kind=kOutput, calls=%fused_computation.42 | convolution fusion | flops 35389440 | bytes 3282948 | tf_op jit(solution)/shard_map/rgc,gcd->rgd/dot_general | solution.py:65
  71.0 0.1 fusion.33
  71.1 1.7 %fusion.12 = bf16[2048,256]{0,1:T(8,128)(2,1)} fusion(bf16[256,512]{0,1:T(8,128)(2,1)S(1)} %fusion.33, bf16[512,2048]{1,0:T(8,128)(2,1)S(1)} %copy-done), kind=kOutput, calls=%fused_computation.12 | convolution fusion | flops 537395200 | bytes 3407872 | tf_op jit(solution)/shard_map/dot_general | solution.py:110
  72.8 23.4 %reduce-scatter.5.cloned.1.call-done = bf16[512,384]{0,1:T(8,128)(2,1)} async-done(((bf16[2048,384]{0,1:T(8,128)(2,1)}), bf16[512,384]{0,1:T(8,128)(2,1)}) %reduce-scatter.5.cloned.1.call-update) | async-done | bytes 393232 | tf_op jit(solution)/shard_map/reduce_scatter | solution.py:118
  96.2 4.6 %all-to-all-start.1 = ((bf16[512,4,96]{0,2,1:T(8,128)(2,1)}), bf16[512,4,96]{0,2,1:T(8,128)(2,1)S(1)}, u32[]{:S(2)}, u32[]{:S(2)}) async-start(bf16[512,4,96]{0,2,1:T(8,128)(2,1)} %bitcast.84), calls=%async_computation.3 | async-start | bytes 786432 | tf_op jit(solution)/shard_map/all_to_all | solution.py:128
  100.8 0.1 copy.25
  100.9 11.4 %all-to-all-done.1 = bf16[512,4,96]{0,2,1:T(8,128)(2,1)S(1)} async-done(((bf16[512,4,96]{0,2,1:T(8,128)(2,1)}), bf16[512,4,96]{0,2,1:T(8,128)(2,1)S(1)}, u32[]{:S(2)}, u32[]{:S(2)}) %all-to-all-start.1) | async-done | bytes 393248 | tf_op jit(solution)/shard_map/all_to_all | solution.py:128
  112.3 1.2 gather_fusion.1
  113.5 0.3 reshape.150
  113.8 1.4 %multiply_reduce_fusion = bf16[512,128]{0,1:T(8,128)(2,1)} fusion(f32[512,128,2]{0,2,1:T(2,128)S(1)} %reshape.150, f32[128,2]{1,0:T(8,128)S(1)} %copy.25), kind=kLoop, calls=%fused_computation.39 | loop fusion | flops 196608 | bytes 656384 | tf_op jit(solution)/shard_map/reduce_sum | solution.py:133
  115.2 8.9 %reduce-scatter.3.cloned.1.call-done = bf16[512,256]{0,1:T(8,128)(2,1)} async-done(((bf16[2048,256]{0,1:T(8,128)(2,1)}), bf16[512,256]{0,1:T(8,128)(2,1)}) %reduce-scatter.3.cloned.1.call-update) | async-done | bytes 262160 | tf_op jit(solution)/shard_map/reduce_scatter | solution.py:109
  (38 shorter events, 1.0 us)
Async XLA Ops:
  7.2 63.9 %copy-start = (bf16[512,2048]{1,0:T(8,128)(2,1)S(1)}, bf16[512,2048]{1,0:T(8,128)(2,1)}, u32[]{:S(2)}) copy-start(bf16[512,2048]{1,0:T(8,128)(2,1)} %param.14) | copy-start | bytes 6291460
  7.2 46.7 %all-gather.2.cloned.1.call-start = ((), (), s32[]{:S(2)}) async-start(), calls=%async_computation.5 | async-start | bytes 1966080 | tf_op jit(solution)/shard_map/all_gather | solution.py:104
  15.0 20.1 %copy-start.1 = (bf16[256,512]{1,0:T(8,128)(2,1)S(1)}, bf16[256,512]{1,0:T(8,128)(2,1)}, u32[]{:S(2)}) copy-start(bf16[256,512]{1,0:T(8,128)(2,1)} %param.11) | copy-start | bytes 786436
  35.0 61.2 %reduce-scatter.5.cloned.1.call-start = ((), (), s32[]{:S(2)}) async-start(), calls=%async_computation.6 | async-start | bytes 1966080 | tf_op jit(solution)/shard_map/reduce_scatter | solution.py:118
  35.1 34.0 %collective-permute-start = (bf16[15,512]{1,0:T(8,128)(2,1)S(1)}, bf16[15,512]{1,0:T(8,128)(2,1)S(1)}, u32[]{:S(2)}, u32[]{:S(2)}) collective-permute-start(bf16[15,512]{1,0:T(8,128)(2,1)S(1)} %slice.43), channel_id=1, source_target_pairs={{0,4},{4,8},{8,12},{1,5},{5,9},{9,13},{2,6},{6,10},{10,14},{3,7},{... | collective-permute-start | bytes 46088 | tf_op jit(solution)/shard_map/ppermute | solution.py:13
  67.9 56.2 %reduce-scatter.3.cloned.1.call-start = ((), (), s32[]{:S(2)}) async-start(), calls=%async_computation.4 | async-start | bytes 1310720 | tf_op jit(solution)/shard_map/reduce_scatter | solution.py:109
  72.8 28.0 %copy-start.2 = (f32[128,2]{0,1:T(2,128)S(1)}, f32[128,2]{0,1:T(2,128)}, u32[]{:S(2)}) copy-start(f32[128,2]{0,1:T(2,128)} %param.18) | copy-start | bytes 3076
  96.2 16.1 %all-to-all-start.1 = ((bf16[512,4,96]{0,2,1:T(8,128)(2,1)}), bf16[512,4,96]{0,2,1:T(8,128)(2,1)S(1)}, u32[]{:S(2)}, u32[]{:S(2)}) async-start(bf16[512,4,96]{0,2,1:T(8,128)(2,1)} %bitcast.84), calls=%async_computation.3 | async-start | bytes 786432 | tf_op jit(solution)/shard_map/all_to_all | solution.py:128
Sparse Core Ops, SparseCore 0:
  35.1 18.7 all-gather.1
  68.1 28.0 reduce-scatter.4
  99.3 24.7 reduce-scatter.2
where the time goes:
time: 131 us
  waiting for transfers between devices  60.4 us (46%)
  blocking collectives  17.9 us (14%)
  matrix products  17.2 us (13%)
  between operations  14 us (11%)
  local copies, waits for them, and re-layouts  7.86 us (6%)
  starting transfers between devices  6.83 us (5%)
  other arithmetic  6.43 us (5%)
    reduce_scatter x1, waiting for transfers between devices, on_device(): lax.psum_scatter(lax.dot_general(weight_cols, hidden, (((0,), (1,)), ((),...  23.4 us
    all_to_all x1, blocking collectives, on_device(): lax.all_to_all(outgoing, 'ep', split_axis=0, concat_axis=0, tiled=True)  17.9 us
    all_gather x1, waiting for transfers between devices, on_device(): section = lax.all_gather(arrived, 'tp', axis=1, tiled=True)  16.7 us
    all_to_all x1, waiting for transfers between devices, on_device(): lax.all_to_all(results, 'ep', split_axis=1, concat_axis=1, tiled=True)  11.4 us
    reduce_scatter x1, waiting for transfers between devices, on_device(): lax.psum_scatter(lax.dot_general(weight_cols, pooled, (((0,), (1,)), ((),...  8.93 us
    dot_general x1, matrix products, on_device(): lax.dot_general(weight_cols, hidden, (((0,), (1,)), ((), ())), preferred_...  8.61 us
    dot_general x1, matrix products, on_device(): gate_pre = jnp.dot(section, w_gate, preferred_element_type=jnp.float32)  5.4 us
    all_to_all x1, starting transfers between devices, on_device(): lax.all_to_all(results, 'ep', split_axis=1, concat_axis=1, tiled=True)  4.6 us
  transfers between devices with their start and end apart: 5, of which 4 were waited for; matrix products, arithmetic and copies ran while one was open for 17% of the time, Pallas kernels for 0%

commit v1 on v0

--- a/solution.py
+++ b/solution.py
@@ -101,7 +101,7 @@
     arrived = lax.all_to_all(outgoing, "ep", split_axis=0, concat_axis=0, tiled=True).reshape(
         arrived_rows, columns
     )
-    section = lax.all_gather(arrived, "tp", axis=1, tiled=True)
+    section = jnp.concatenate(lax.all_gather(arrived, "tp"), axis=1)
     gate_pre = jnp.dot(section, w_gate, preferred_element_type=jnp.float32)
     up_pre = jnp.dot(section, w_up, preferred_element_type=jnp.float32)
     hidden = (jax.nn.silu(gate_pre) * up_pre).astype(jnp.bfloat16)

time: 131 us -> 134 us (1.023)
  local copies, waits for them, and re-layouts: 7.86 us -> 10.4 us
    all_gather x0 -> x1, local copies, waits for them, and re-layouts: none -> 2.59 us  [on_device(): section = jnp.concatenate(lax.all_gather(arrived, 'tp'), axis=1)]
  transfers between devices with their start and end apart: 5 -> 5, of which waited for: 4 -> 4; matrix products, arithmetic and copies ran while one was open for 17% -> 18% of each run, Pallas kernels for 0% -> 0%
where the time goes in v1:
time: 134 us; the launch traced here: 133 us
  waiting for transfers between devices  60.4 us (45%)
  blocking collectives  17.9 us (13%)
  matrix products  17.3 us (13%)
  between operations  14 us (10%)
  local copies, waits for them, and re-layouts  10.4 us (8%)
  starting transfers between devices  6.84 us (5%)
  other arithmetic  6.43 us (5%)
    reduce_scatter x1, waiting for transfers between devices, on_device(): lax.psum_scatter(lax.dot_general(weight_cols, hidden, (((0,), (1,)), ((),...  23.4 us
    all_to_all x1, blocking collectives, on_device(): lax.all_to_all(outgoing, 'ep', split_axis=0, concat_axis=0, tiled=True)  17.9 us
    all_gather x1, waiting for transfers between devices, on_device(): section = jnp.concatenate(lax.all_gather(arrived, 'tp'), axis=1)  16.7 us
    all_to_all x1, waiting for transfers between devices, on_device(): lax.all_to_all(results, 'ep', split_axis=1, concat_axis=1, tiled=True)  11.4 us
    reduce_scatter x1, waiting for transfers between devices, on_device(): lax.psum_scatter(lax.dot_general(weight_cols, pooled, (((0,), (1,)), ((),...  8.93 us
    dot_general x1, matrix products, on_device(): lax.dot_general(weight_cols, hidden, (((0,), (1,)), ((), ())), preferred_...  8.7 us
    dot_general x1, matrix products, on_device(): gate_pre = jnp.dot(section, w_gate, preferred_element_type=jnp.float32)  5.42 us
    all_to_all x1, starting transfers between devices, on_device(): lax.all_to_all(results, 'ep', split_axis=1, concat_axis=1, tiled=True)  4.6 us
  transfers between devices with their start and end apart: 5, of which 4 were waited for; matrix products, arithmetic and copies ran while one was open for 18% of the time, Pallas kernels for 0%

profile of v1, /device:TPU:0, one launch (start us, length us, event | category | flops | bytes accessed | tf_op | source)
XLA Modules:
  0.0 133.4 jit_solution(10331654955853851028)
XLA Ops:
  7.2 0.9 copy.39
  8.2 0.1 eq.97
  8.3 0.1 eq.93
  8.4 0.7 broadcast_multiply_fusion
  9.1 1.2 fusion.19
  10.4 1.2 reduce-window.6
  11.6 0.1 slice.72
  11.7 0.1 copy.41
  11.8 0.1 copy.42
  12.0 0.1 copy.38
  12.1 0.1 mul.84
  12.3 1.4 %scatter_custom_fusion = s32[384]{0:T(512)S(1)} fusion(s32[256]{0:T(256)S(1)} %bitcast.91, s32[256]{0:T(256)S(1)} %and_select_fusion, s32[]{:T(128)} %constant.80.clone.1), kind=kCustom, calls=%fused_computation.66 | custom fusion | bytes 1540 | tf_op jit(solution)/shard_map/scatter | solution.py:92
  13.7 1.2 fusion.21
  15.0 2.1 %gather_fusion = bf16[384,512]{1,0:T(8,128)(2,1)S(1)} fusion(bf16[129,512]{1,0:T(8,128)(2,1)S(1)} %pad_dynamic-slice_fusion, s32[1024]{0:T(1024)S(1)} %pad_clamp_fusion.1), kind=kCustom, calls=%fused_computation | custom fusion | bytes 787968 | tf_op jit(solution)/shard_map/gather | solution.py:100
  17.1 17.9 %all_to_all.10 = bf16[4,96,512]{2,1,0:T(8,128)(2,1)} all-to-all(bf16[4,96,512]{2,1,0:T(8,128)(2,1)S(1)} %bitcast.88), channel_id=1, replica_groups=mesh['grp'=2,'ep'=4,'tp'=4] {'ep'}, dimensions={0} | all-to-all | bytes 786432 | tf_op jit(solution)/shard_map/all_to_all | solution.py:101
  35.1 2.1 %collective-permute-start = (bf16[15,512]{1,0:T(8,128)(2,1)S(1)}, bf16[15,512]{1,0:T(8,128)(2,1)S(1)}, u32[]{:S(2)}, u32[]{:S(2)}) collective-permute-start(bf16[15,512]{1,0:T(8,128)(2,1)S(1)} %slice.43), channel_id=1, source_target_pairs={{0,4},{4,8},{8,12},{1,5},{5,9},{9,13},{2,6},{6,10},{10,14},{3,7},{... | collective-permute-start | bytes 46088 | tf_op jit(solution)/shard_map/ppermute | solution.py:13
  37.2 16.7 %all-gather.2.cloned.1.call-done = bf16[4,384,512]{2,1,0:T(8,128)(2,1)} async-done(((bf16[1,384,512]{2,1,0:T(8,128)(2,1)}), bf16[4,384,512]{2,1,0:T(8,128)(2,1)}) %all-gather.2.cloned.1.call-update) | async-done | bytes 1572880 | tf_op jit(solution)/shard_map/all_gather | solution.py:104
  53.9 2.6 %copy.43 = bf16[4,384,512]{1,2,0:T(8,128)(2,1)} copy(bf16[4,384,512]{2,1,0:T(8,128)(2,1)} %all-gather.2.cloned.1.call-done) | data formatting | bytes 3145728 | tf_op jit(solution)/shard_map/all_gather | solution.py:104
  56.5 5.4 %fusion.4 = f32[384,896]{1,0:T(8,128)} fusion(bf16[384,2048]{0,1:T(8,128)(2,1)} %bitcast.85, bf16[1,2048,896]{2,1,0:T(8,128)(2,1)} %param.19), kind=kOutput, calls=%fused_computation.7 | convolution fusion | flops 1409286144 | bytes 6619136 | tf_op jit(solution)/shard_map/dot_general | solution.py:105
  61.9 8.7 %fusion.9 = bf16[2048,384]{0,1:T(8,128)(2,1)} fusion(bf16[1,896,2048]{2,1,0:T(8,128)(2,1)} %param.21, bf16[384,2048]{0,1:T(8,128)(2,1)} %bitcast.86, bf16[1,2048,896]{2,1,0:T(8,128)(2,1)} %param.20, f32[384,896]{1,0:T(8,128)} %fusion.4), kind=kOutput, calls=%fused_computation.10 | convolution fusion | flops 2821423104 | bytes 11862016 | tf_op jit(solution)/shard_map/dot_general | solution.py:119
  71.1 0.8 dynamic_slice.10
  72.1 1.5 %fusion.35 = f32[4,128,256]{2,1,0:T(8,128)S(1)} fusion(bf16[16,128,128]{2,1,0:T(8,128)(2,1)} %param.12, s32[]{:T(128)S(6)} %select_n.46, f32[256]{0:T(256)S(1)} %get-tuple-element.2, f32[270,512]{1,0:T(8,128)S(1)} %slice_add_fusion.1, pred[512]{0:T(512)(128)(4,1)S(1)} %broadcast_bitcast_fusion, f32[256]{0:T(256)S(1)} %get-tuple-element.3, ...), kind=kOutput, calls=%fused_computation.42 | convolution fusion | flops 35389440 | bytes 3282948 | tf_op jit(solution)/shard_map/rgc,gcd->rgd/dot_general | solution.py:65
  73.7 0.1 fusion.33
  73.8 1.7 %fusion.12 = bf16[2048,256]{0,1:T(8,128)(2,1)} fusion(bf16[256,512]{0,1:T(8,128)(2,1)S(1)} %fusion.33, bf16[512,2048]{1,0:T(8,128)(2,1)S(1)} %copy-done), kind=kOutput, calls=%fused_computation.12 | convolution fusion | flops 537395200 | bytes 3407872 | tf_op jit(solution)/shard_map/dot_general | solution.py:110
  75.5 23.4 %reduce-scatter.5.cloned.1.call-done = bf16[512,384]{0,1:T(8,128)(2,1)} async-done(((bf16[2048,384]{0,1:T(8,128)(2,1)}), bf16[512,384]{0,1:T(8,128)(2,1)}) %reduce-scatter.5.cloned.1.call-update) | async-done | bytes 393232 | tf_op jit(solution)/shard_map/reduce_scatter | solution.py:118
  98.9 4.6 %all-to-all-start.1 = ((bf16[512,4,96]{0,2,1:T(8,128)(2,1)}), bf16[512,4,96]{0,2,1:T(8,128)(2,1)S(1)}, u32[]{:S(2)}, u32[]{:S(2)}) async-start(bf16[512,4,96]{0,2,1:T(8,128)(2,1)} %bitcast.89), calls=%async_computation.3 | async-start | bytes 786432 | tf_op jit(solution)/shard_map/all_to_all | solution.py:128
  103.5 0.1 copy.44
  103.6 11.4 %all-to-all-done.1 = bf16[512,4,96]{0,2,1:T(8,128)(2,1)S(1)} async-done(((bf16[512,4,96]{0,2,1:T(8,128)(2,1)}), bf16[512,4,96]{0,2,1:T(8,128)(2,1)S(1)}, u32[]{:S(2)}, u32[]{:S(2)}) %all-to-all-start.1) | async-done | bytes 393248 | tf_op jit(solution)/shard_map/all_to_all | solution.py:128
  115.0 1.2 gather_fusion.1
  116.2 0.3 reshape.154
  116.5 1.4 %multiply_reduce_fusion = bf16[512,128]{0,1:T(8,128)(2,1)} fusion(f32[512,128,2]{0,2,1:T(2,128)S(1)} %reshape.154, f32[128,2]{1,0:T(8,128)S(1)} %copy.44), kind=kLoop, calls=%fused_computation.39 | loop fusion | flops 196608 | bytes 656384 | tf_op jit(solution)/shard_map/reduce_sum | solution.py:133
  117.9 8.9 %reduce-scatter.3.cloned.1.call-done = bf16[512,256]{0,1:T(8,128)(2,1)} async-done(((bf16[2048,256]{0,1:T(8,128)(2,1)}), bf16[512,256]{0,1:T(8,128)(2,1)}) %reduce-scatter.3.cloned.1.call-update) | async-done | bytes 262160 | tf_op jit(solution)/shard_map/reduce_scatter | solution.py:109
  (39 shorter events, 1.1 us)
Async XLA Ops:
  7.2 66.6 %copy-start = (bf16[512,2048]{1,0:T(8,128)(2,1)S(1)}, bf16[512,2048]{1,0:T(8,128)(2,1)}, u32[]{:S(2)}) copy-start(bf16[512,2048]{1,0:T(8,128)(2,1)} %param.14) | copy-start | bytes 6291460
  7.2 46.7 %all-gather.2.cloned.1.call-start = ((), (), s32[]{:S(2)}) async-start(), calls=%async_computation.5 | async-start | bytes 1966080 | tf_op jit(solution)/shard_map/all_gather | solution.py:104
  15.0 20.1 %copy-start.1 = (bf16[256,512]{1,0:T(8,128)(2,1)S(1)}, bf16[256,512]{1,0:T(8,128)(2,1)}, u32[]{:S(2)}) copy-start(bf16[256,512]{1,0:T(8,128)(2,1)} %param.11) | copy-start | bytes 786436
  35.0 63.9 %reduce-scatter.5.cloned.1.call-start = ((), (), s32[]{:S(2)}) async-start(), calls=%async_computation.6 | async-start | bytes 1966080 | tf_op jit(solution)/shard_map/reduce_scatter | solution.py:118
  35.1 36.7 %collective-permute-start = (bf16[15,512]{1,0:T(8,128)(2,1)S(1)}, bf16[15,512]{1,0:T(8,128)(2,1)S(1)}, u32[]{:S(2)}, u32[]{:S(2)}) collective-permute-start(bf16[15,512]{1,0:T(8,128)(2,1)S(1)} %slice.43), channel_id=1, source_target_pairs={{0,4},{4,8},{8,12},{1,5},{5,9},{9,13},{2,6},{6,10},{10,14},{3,7},{... | collective-permute-start | bytes 46088 | tf_op jit(solution)/shard_map/ppermute | solution.py:13
  70.6 56.2 %reduce-scatter.3.cloned.1.call-start = ((), (), s32[]{:S(2)}) async-start(), calls=%async_computation.4 | async-start | bytes 1310720 | tf_op jit(solution)/shard_map/reduce_scatter | solution.py:109
  75.5 28.0 %copy-start.2 = (f32[128,2]{0,1:T(2,128)S(1)}, f32[128,2]{0,1:T(2,128)}, u32[]{:S(2)}) copy-start(f32[128,2]{0,1:T(2,128)} %param.18) | copy-start | bytes 3076
  98.9 16.1 %all-to-all-start.1 = ((bf16[512,4,96]{0,2,1:T(8,128)(2,1)}), bf16[512,4,96]{0,2,1:T(8,128)(2,1)S(1)}, u32[]{:S(2)}, u32[]{:S(2)}) async-start(bf16[512,4,96]{0,2,1:T(8,128)(2,1)} %bitcast.89), calls=%async_computation.3 | async-start | bytes 786432 | tf_op jit(solution)/shard_map/all_to_all | solution.py:128
Sparse Core Ops, SparseCore 0:
  35.1 18.7 all-gather.1
  70.8 28.0 reduce-scatter.4
  102.0 24.7 reduce-scatter.2
